TPU v7x, 32 devices: a whole 2x2x4 slice. The times are simulated.
32 devices in a mesh: grp: 1, ep: 16 (over z, y, x), tp: 2 (over core).
Axes of the slice: x: 2, y: 2, z: 4, core: 2. Of those that a mesh axis runs over, the one named last changes fastest.
Arguments:
- tokens_in: bfloat16 [1024, 2048], P(('grp', 'ep')), may hold values from -6 to 6
- norm_gain: float32 [2048], replicated, may hold values from 0.1 to 1.9
- gate_proj: bfloat16 [16, 2048, 1024], P('ep', None, 'tp'), may hold values from -0.125 to 0.125
- up_proj: bfloat16 [16, 2048, 1024], P('ep', None, 'tp'), may hold values from -0.125 to 0.125
- down_proj: bfloat16 [16, 1024, 2048], P('ep', 'tp'), may hold values from -0.1875 to 0.1875
- route_ids: int32 [1024, 8], P(('grp', 'ep')), may hold values from 0 to 15, all different within a row; in each aligned block of 64 rows (0 to 63, 64 to 127, ...) at most 64 rows name the same one
- group_weight: float32 [1024, 2], P(('grp', 'ep')), may hold values from 0.05 to 1
- expert_weight: float32 [1024, 8], P(('grp', 'ep')), may hold values from 0.05 to 1
Outputs:
- expert_mix: bfloat16 [1024, 2048], P(('grp', 'ep'), 'tp')
Inputs may be any that keep to these rules, and one draw needn't show every extreme that they name: `route_ids`: each row names 8 different experts; within the rows of one index of ep no expert is named by more than 64 rows, a bound that some of them reach.
All inputs are finite; a program needn't handle non-finite values.
Results may differ from a plain program's by a relative error of at most 0.0077.
Values may be sent and summed in bfloat16 or wider, within the bound.
A program may use at most 64 MiB of HBM per device.

v0:
```python
import jax
import jax.numpy as jnp
from jax import lax
from jax.sharding import PartitionSpec as P

TOP = 8
EXP_GRP = 8


EPSILON = 1e-06


def on_device(
    tokens_in, norm_gain, gate_proj, up_proj, down_proj, route_ids, group_weight, expert_weight
):
    token_count, model_width = tokens_in.shape
    expert_count = gate_proj.shape[0] * lax.axis_size("ep")
    lane_count = lax.axis_size("tp")
    part_width = model_width // lane_count
    capacity = min(token_count, max(2, 2 * token_count * TOP // expert_count))
    slot_total = expert_count * capacity
    row_values = tokens_in.astype(jnp.float32)
    inv_scale = lax.rsqrt(jnp.mean(row_values * row_values, axis=-1, keepdims=True) + EPSILON)
    normed = (row_values * inv_scale * norm_gain).astype(jnp.bfloat16)
    route_count = token_count * TOP
    flat_ids = route_ids.reshape(route_count)
    positions = jnp.arange(route_count, dtype=jnp.int32)
    same_expert = (flat_ids[:, None] == flat_ids[None, :]) & (
        positions[None, :] < positions[:, None]
    )
    slot_rank = jnp.sum(same_expert.astype(jnp.int32), axis=1)
    slot_index = flat_ids * capacity + slot_rank
    slot_match = jnp.arange(slot_total, dtype=jnp.int32)[:, None] == slot_index[None, :]
    selector = jnp.sum(
        slot_match.reshape(slot_total, token_count, TOP).astype(jnp.int32), axis=2
    ).astype(jnp.bfloat16)
    gate_local = gate_proj[0]
    up_local = up_proj[0]
    lane_index = lax.axis_index("tp")
    own_half = lax.dynamic_slice_in_dim(normed, lane_index * part_width, part_width, 1)
    outgoing = jnp.dot(selector, own_half, preferred_element_type=jnp.float32).astype(jnp.bfloat16)
    arrived = lax.all_to_all(
        outgoing.reshape(expert_count, capacity, part_width),
        "ep",
        split_axis=0,
        concat_axis=0,
        tiled=True,
    )
    arrived = arrived.reshape(slot_total, part_width)
    column_piece = lax.all_gather(arrived, "tp", axis=1, tiled=True)
    gate_acts = jnp.dot(column_piece, gate_local, preferred_element_type=jnp.float32)
    up_acts = jnp.dot(column_piece, up_local, preferred_element_type=jnp.float32)
    hidden = (jax.nn.silu(gate_acts) * up_acts).astype(jnp.bfloat16)
    partial_rows = jnp.dot(hidden, down_proj[0], preferred_element_type=jnp.float32)
    summed = lax.psum_scatter(
        partial_rows.reshape(expert_count, capacity, model_width).astype(jnp.bfloat16),
        "tp",
        scatter_dimension=2,
        tiled=True,
    )
    returned = lax.all_to_all(summed, "ep", split_axis=0, concat_axis=0, tiled=True).reshape(
        slot_total, part_width
    )
    picked = returned[slot_index].astype(jnp.float32).reshape(token_count, TOP, part_width)
    group_ids = route_ids // EXP_GRP
    group_count = group_weight.shape[1]
    group_match = (
        group_ids[:, :, None] == jnp.arange(group_count, dtype=jnp.int32)[None, None, :]
    ).astype(jnp.float32)
    group_part = jnp.sum(group_weight[:, None, :] * group_match, axis=2)
    gate_values = group_part * expert_weight / jnp.sum(expert_weight, axis=1, keepdims=True)
    return jnp.sum(picked * gate_values[:, :, None], axis=1).astype(jnp.bfloat16)


def solution(mesh):
    in_specs = (
        P(("grp", "ep"), None),
        P(),
        P("ep", None, "tp"),
        P("ep", None, "tp"),
        P("ep", "tp", None),
        P(("grp", "ep"), None),
        P(("grp", "ep"), None),
        P(("grp", "ep"), None),
    )
    out_specs = P(("grp", "ep"), "tp")
    return jax.shard_map(
        on_device, mesh=mesh, in_specs=in_specs, out_specs=out_specs, check_vma=False
    )
```

profile of v0, /device:TPU:12, one launch (start us, length us, event | category | flops | bytes accessed | tf_op | source)
XLA Modules:
  0.0 173.9 jit_solution(4123312563667947729)
XLA Ops:
  6.5 0.0 copy-start
  6.5 0.0 all-gather.2.cloned.1.call-start
  6.5 1.1 convert_element_type.38
  7.7 1.1 multiply_reduce_fusion
  8.8 0.8 copy.18
  9.6 0.1 eq.43
  9.7 0.3 convert_reduce_fusion.1
  9.9 0.1 reduce_sum.59
  10.0 0.7 convert_reduce_fusion
  10.7 0.7 dynamic-slice
  11.4 0.8 convolution_convert_fusion.1
  12.2 54.7 %all_to_all.10 = bf16[16,64,1024]{2,1,0:T(8,128)(2,1)} all-to-all(bf16[16,64,1024]{2,1,0:T(8,128)(2,1)S(1)} %bitcast.25), channel_id=1, replica_groups=mesh['grp'=1,'ep'=16,'tp'=2] {'ep'}, dimensions={0} | all-to-all | bytes 4194304 | tf_op jit(solution)/shard_map/all_to_all | solution.py:42
  66.9 0.0 all-gather.2.cloned.1.call-update
  66.9 0.0 reduce-scatter.2.cloned.1.call-start
  67.0 13.1 %all-gather.2.cloned.1.call-done = bf16[1024,2048]{1,0:T(8,128)(2,1)} async-done(((bf16[1024,1024]{1,0:T(8,128)(2,1)}), bf16[1024,2048]{1,0:T(8,128)(2,1)}) %all-gather.2.cloned.1.call-update) | async-done | bytes 4194320 | tf_op jit(solution)/shard_map/all_gather | solution.py:50
  80.0 0.0 copy-start.4
  80.1 0.0 copy-start.5
  80.1 5.3 %fusion.2 = f32[1024,512]{1,0:T(8,128)S(1)} fusion(bf16[1024,2048]{1,0:T(8,128)(2,1)} %all-gather.2.cloned.1.call-done, bf16[1,2048,512]{2,1,0:T(8,128)(2,1)} %param.11), kind=kOutput, calls=%fused_computation.5 | convolution fusion | flops 2147483648 | bytes 8388608 | tf_op jit(solution)/shard_map/dot_general | solution.py:52
  85.4 0.0 copy-done.4
  85.4 0.0 copy-done.5
  85.4 2.6 %multiply_convert_fusion = bf16[1024,512]{1,0:T(8,128)(2,1)S(1)} fusion(f32[1024,512]{1,0:T(8,128)S(1)} %fusion.2, bf16[1024,2048]{1,0:T(8,128)(2,1)S(1)} %copy-done.4, bf16[1,2048,512]{2,1,0:T(8,128)(2,1)S(1)} %copy-done.5), kind=kOutput, calls=%fused_computation.9 | convolution fusion | flops 2150629376 | bytes 9437184 | tf_op jit(solution)/shard_map/dot_general | solution.py:51
  88.1 0.0 copy-done
  88.1 4.3 %convolution_convert_fusion = bf16[16,64,2048]{2,1,0:T(8,128)(2,1)} fusion(bf16[16,64,512]{2,1,0:T(8,128)(2,1)S(1)} %bitcast.28, bf16[1,512,2048]{2,1,0:T(8,128)(2,1)S(1)} %copy-done), kind=kOutput, calls=%fused_computation.1 | convolution fusion | flops 2149580800 | bytes 7340032 | tf_op jit(solution)/shard_map/dot_general | solution.py:54
  92.3 0.0 reduce-scatter.2.cloned.1.call-update
  92.4 0.0 copy-start.1
  92.4 0.0 copy-start.2
  92.4 0.0 copy-start.3
  92.4 13.3 %reduce-scatter.2.cloned.1.call-done = bf16[16,64,1024]{2,1,0:T(8,128)(2,1)} async-done(((bf16[16,64,2048]{2,1,0:T(8,128)(2,1)}), bf16[16,64,1024]{2,1,0:T(8,128)(2,1)}) %reduce-scatter.2.cloned.1.call-update) | async-done | bytes 2097168 | tf_op jit(solution)/shard_map/reduce_scatter | solution.py:55
  105.7 7.0 %all-to-all-start.1 = ((bf16[16,64,1024]{2,1,0:T(8,128)(2,1)}), bf16[16,64,1024]{2,1,0:T(8,128)(2,1)}, u32[]{:S(2)}, u32[]{:S(2)}) async-start(bf16[16,64,1024]{2,1,0:T(8,128)(2,1)} %reduce-scatter.2.cloned.1.call-done), calls=%async_computation.2 | async-start | bytes 4194304 | tf_op jit(solution)/shard_map/all_to_all | solution.py:61
  112.6 0.1 mul.78
  112.7 0.0 copy-done.1
  112.8 0.0 copy-done.2
  112.8 0.0 copy-done.3
  112.8 0.1 copy.20
  112.9 48.2 %all-to-all-done.1 = bf16[16,64,1024]{2,1,0:T(8,128)(2,1)} async-done(((bf16[16,64,1024]{2,1,0:T(8,128)(2,1)}), bf16[16,64,1024]{2,1,0:T(8,128)(2,1)}, u32[]{:S(2)}, u32[]{:S(2)}) %all-to-all-start.1) | async-done | bytes 2097184 | tf_op jit(solution)/shard_map/all_to_all | solution.py:61
  161.1 4.6 %gather_fusion = bf16[512,1024]{1,0:T(8,128)(2,1)S(1)} fusion(bf16[1024,1024]{1,0:T(8,128)(2,1)} %bitcast.7, s32[1024]{0:T(1024)S(1)} %pad_clamp_fusion), kind=kCustom, calls=%fused_computation | custom fusion | bytes 2099200 | tf_op jit(solution)/shard_map/gather | solution.py:64
  165.7 1.4 fusion
  (8 shorter events, 0.1 us)
Async XLA Ops:
  6.5 81.5 %copy-start = (bf16[1,512,2048]{2,1,0:T(8,128)(2,1)S(1)}, bf16[1,512,2048]{2,1,0:T(8,128)(2,1)}, u32[]{:S(2)}) copy-start(bf16[1,512,2048]{2,1,0:T(8,128)(2,1)} %param.12) | copy-start | bytes 6291460
  6.5 73.5 %all-gather.2.cloned.1.call-start = ((), (), s32[]{:S(2)}) async-start(), calls=%async_computation.3 | async-start | bytes 6291456 | tf_op jit(solution)/shard_map/all_gather | solution.py:50
  66.9 38.8 %reduce-scatter.2.cloned.1.call-start = ((), (), s32[]{:S(2)}) async-start(), calls=%async_computation.4 | async-start | bytes 6291456 | tf_op jit(solution)/shard_map/reduce_scatter | solution.py:55
  80.0 5.3 %copy-start.4 = (bf16[1024,2048]{1,0:T(8,128)(2,1)S(1)}, bf16[1024,2048]{1,0:T(8,128)(2,1)}, u32[]{:S(2)}) copy-start(bf16[1024,2048]{1,0:T(8,128)(2,1)} %all-gather.2.cloned.1.call-done) | copy-start | bytes 12582916
  80.1 5.3 %copy-start.5 = (bf16[1,2048,512]{2,1,0:T(8,128)(2,1)S(1)}, bf16[1,2048,512]{2,1,0:T(8,128)(2,1)}, u32[]{:S(2)}) copy-start(bf16[1,2048,512]{2,1,0:T(8,128)(2,1)} %param.10) | copy-start | bytes 6291460
  92.4 20.4 %copy-start.1 = (f32[64,8]{0,1:T(8,128)S(1)}, f32[64,8]{0,1:T(8,128)}, u32[]{:S(2)}) copy-start(f32[64,8]{0,1:T(8,128)} %param.15) | copy-start | bytes 6148
  92.4 20.4 %copy-start.2 = (s32[64,8]{0,1:T(8,128)S(1)}, s32[64,8]{0,1:T(8,128)}, u32[]{:S(2)}) copy-start(s32[64,8]{0,1:T(8,128)} %param.13) | copy-start | bytes 6148
  92.4 20.4 %copy-start.3 = (f32[64,2]{0,1:T(2,128)S(1)}, f32[64,2]{0,1:T(2,128)}, u32[]{:S(2)}) copy-start(f32[64,2]{0,1:T(2,128)} %param.14) | copy-start | bytes 1540
  105.7 55.4 %all-to-all-start.1 = ((bf16[16,64,1024]{2,1,0:T(8,128)(2,1)}), bf16[16,64,1024]{2,1,0:T(8,128)(2,1)}, u32[]{:S(2)}, u32[]{:S(2)}) async-start(bf16[16,64,1024]{2,1,0:T(8,128)(2,1)} %reduce-scatter.2.cloned.1.call-done), calls=%async_computation.2 | async-start | bytes 4194304 | tf_op jit(solution)/shard_map/all_to_all | solution.py:61
Sparse Core Ops, SparseCore 0:
  67.0 12.9 all-gather.1
  92.5 13.1 reduce-scatter.1
where the time goes:
time: 174 us
  waiting for transfers between devices  74.6 us (43%)
  blocking collectives  54.7 us (31%)
  between operations  13.6 us (8%)
  matrix products  13 us (7%)
  starting transfers between devices  7.01 us (4%)
  local copies, waits for them, and re-layouts  6.44 us (4%)
  other arithmetic  4.59 us (3%)
    all_to_all x1, blocking collectives, on_device(): lax.all_to_all(outgoing.reshape(expert_count, capacity, part_width), 'ep'...  54.7 us
    all_to_all x1, waiting for transfers between devices, on_device(): lax.all_to_all(summed, 'ep', split_axis=0, concat_axis=0, tiled=True)  48.2 us
    reduce_scatter x1, waiting for transfers between devices, on_device(): lax.psum_scatter(partial_rows.reshape(expert_count, capacity, model_width...  13.3 us
    all_gather x1, waiting for transfers between devices, on_device(): column_piece = lax.all_gather(arrived, 'tp', axis=1, tiled=True)  13.1 us
    all_to_all x1, starting transfers between devices, on_device(): lax.all_to_all(summed, 'ep', split_axis=0, concat_axis=0, tiled=True)  6.97 us
    dot_general x1, matrix products, on_device(): jnp.dot(column_piece, up_local, preferred_element_type=jnp.float32)  5.32 us
    gather x1, local copies, waits for them, and re-layouts, on_device(): returned[slot_index].astype(jnp.float32)  4.59 us
    dot_general x1, matrix products, on_device(): jnp.dot(hidden, down_proj[0], preferred_element_type=jnp.float32)  4.27 us
  transfers between devices with their start and end apart: 3, of which 3 were waited for; matrix products, arithmetic and copies ran while one was open for 0% of the time, Pallas kernels for 0%

commit v1 on v0

v1 whole, which is shorter than its diff:
```python
import jax
import jax.numpy as jnp
from jax import lax
from jax.sharding import PartitionSpec as P

EXP_GRP = 8


EPSILON = 1e-06


def on_device(
    tokens_in, norm_gain, gate_proj, up_proj, down_proj, route_ids, group_weight, expert_weight
):
    token_count, model_width = tokens_in.shape
    expert_count = gate_proj.shape[0] * lax.axis_size("ep")
    lane_count = lax.axis_size("tp")
    lane_index = lax.axis_index("tp")
    share = token_count // lane_count
    own_rows = lax.dynamic_slice_in_dim(tokens_in, lane_index * share, share, 0)
    row_values = own_rows.astype(jnp.float32)
    inv_scale = lax.rsqrt(jnp.mean(row_values * row_values, axis=-1, keepdims=True) + EPSILON)
    normed = (row_values * inv_scale * norm_gain).astype(jnp.bfloat16)
    rows = lax.all_gather(normed, ("ep", "tp"), axis=0, tiled=True)
    experts = jnp.arange(expert_count, dtype=jnp.int32)
    share_of = expert_weight / jnp.sum(expert_weight, axis=1, keepdims=True)
    named = route_ids[:, :, None] == experts[None, None, :]
    chosen = jnp.sum(jnp.where(named, share_of[:, :, None], 0.0), axis=1)
    gates = chosen * jnp.repeat(group_weight, EXP_GRP, axis=1)
    all_gates = lax.all_gather(gates, "ep", axis=0, tiled=True)
    own_gate = lax.dynamic_slice_in_dim(all_gates, lax.axis_index("ep"), 1, 1)
    gate_acts = jnp.dot(rows, gate_proj[0], preferred_element_type=jnp.float32)
    up_acts = jnp.dot(rows, up_proj[0], preferred_element_type=jnp.float32)
    hidden = (jax.nn.silu(gate_acts) * up_acts).astype(jnp.bfloat16)
    partial_rows = jnp.dot(hidden, down_proj[0], preferred_element_type=jnp.float32)
    weighted = (partial_rows * own_gate).astype(jnp.bfloat16)
    halves = lax.psum_scatter(weighted, "tp", scatter_dimension=1, tiled=True)
    return lax.psum_scatter(halves, "ep", scatter_dimension=0, tiled=True)


def solution(mesh):
    in_specs = (
        P(("grp", "ep"), None),
        P(),
        P("ep", None, "tp"),
        P("ep", None, "tp"),
        P("ep", "tp", None),
        P(("grp", "ep"), None),
        P(("grp", "ep"), None),
        P(("grp", "ep"), None),
    )
    out_specs = P(("grp", "ep"), "tp")
    return jax.shard_map(
        on_device, mesh=mesh, in_specs=in_specs, out_specs=out_specs, check_vma=False
    )
```

time: 174 us -> 194 us (1.11)
  the two profiles are of different devices: /device:TPU:12 before, /device:TPU:0 now
where the time goes in v1:
time: 194 us
  waiting for transfers between devices  115 us (59%)
  blocking collectives  43.3 us (22%)
  matrix products  16.6 us (9%)
  between operations  13.1 us (7%)
  other arithmetic  5.67 us (3%)
    reduce_scatter x1, waiting for transfers between devices, on_device(): return lax.psum_scatter(halves, 'ep', scatter_dimension=0, tiled=True)  85.1 us
    all_gather x1, blocking collectives, on_device(): all_gates = lax.all_gather(gates, 'ep', axis=0, tiled=True)  43.3 us
    all_gather x1, waiting for transfers between devices, on_device(): rows = lax.all_gather(normed, ('ep', 'tp'), axis=0, tiled=True)  19.2 us
    reduce_scatter x1, waiting for transfers between devices, on_device(): halves = lax.psum_scatter(weighted, 'tp', scatter_dimension=1, tiled=True)  10.8 us
    dot_general x1, matrix products, on_device(): jnp.dot(hidden, down_proj[0], preferred_element_type=jnp.float32)  10.1 us
    dot_general x1, matrix products, on_device(): up_acts = jnp.dot(rows, up_proj[0], preferred_element_type=jnp.float32)  6.59 us
  transfers between devices with their start and end apart: 3, of which 3 were waited for; matrix products, arithmetic and copies ran while one was open for 2% of the time, Pallas kernels for 0%

profile of v1, /device:TPU:0, one launch (start us, length us, event | category | flops | bytes accessed | tf_op | source)
XLA Modules:
  0.0 194.1 jit_solution(4281065118066478844)
XLA Ops:
  6.5 0.0 copy-start
  6.5 0.0 all-gather.3.cloned.1.call-start
  6.5 1.2 fusion.9
  7.7 1.7 fusion.11
  9.4 0.0 all-gather.3.cloned.1.call-update
  9.4 0.0 reduce-scatter.3.cloned.1.call-start
  9.5 0.7 reduce_sum.28
  10.2 0.7 broadcast_divide_fusion
  10.9 0.7 select_reduce_fusion
  11.6 0.7 fusion.12
  12.3 43.3 %all-gather = f32[16,64,16]{1,2,0:T(8,128)S(1)} all-gather(f32[1,64,16]{1,2,0:T(8,128)S(1)} %fusion.12), channel_id=1, replica_groups=mesh['grp'=1,'ep'=16,'tp'=2] {'ep'}, dimensions={0}, use_global_device_ids=true | all-gather | bytes 69632 | tf_op jit(solution)/shard_map/all_gather | solution.py:30
  55.7 0.1 reshape.17
  55.8 19.2 %all-gather.3.cloned.1.call-done = bf16[1024,2048]{1,0:T(8,128)(2,1)} async-done(((bf16[32,2048]{1,0:T(8,128)(2,1)}), bf16[1024,2048]{1,0:T(8,128)(2,1)}) %all-gather.3.cloned.1.call-update) | async-done | bytes 4194320 | tf_op jit(solution)/shard_map/all_gather | solution.py:24
  75.0 6.6 %fusion.1 = f32[1024,512]{1,0:T(8,128)} fusion(bf16[1024,2048]{1,0:T(8,128)(2,1)} %all-gather.3.cloned.1.call-done, bf16[1,2048,512]{2,1,0:T(8,128)(2,1)} %param.11), kind=kOutput, calls=%fused_computation.2 | convolution fusion | flops 2147483648 | bytes 8388608 | tf_op jit(solution)/shard_map/dot_general | solution.py:33
  81.5 0.0 copy-done
  81.5 10.1 %multiply_convert_fusion = bf16[1024,2048]{1,0:T(8,128)(2,1)} fusion(f32[1024]{0:T(1024)S(1)} %bitcast.24, bf16[1,512,2048]{2,1,0:T(8,128)(2,1)S(1)} %copy-done, f32[1024,512]{1,0:T(8,128)} %fusion.1, bf16[1024,2048]{1,0:T(8,128)(2,1)} %all-gather.3.cloned.1.call-done, bf16[1,2048,512]{2,1,0:T(8,128)(2,1)} %param.10), kind=kOutput, calls=%fused_computation | convolution fusion | flops 4302307328 | bytes 14684160 | tf_op jit(solution)/shard_map/dot_general | solution.py:35
  91.6 0.0 reduce-scatter.3.cloned.1.call-update
  91.6 0.0 reduce-scatter.5.cloned.1.call-start
  91.7 10.8 %reduce-scatter.3.cloned.1.call-done = bf16[1024,1024]{1,0:T(8,128)(2,1)} async-done(((bf16[1024,2048]{1,0:T(8,128)(2,1)}), bf16[1024,1024]{1,0:T(8,128)(2,1)}) %reduce-scatter.3.cloned.1.call-update) | async-done | bytes 2097168 | tf_op jit(solution)/shard_map/reduce_scatter | solution.py:37
  102.4 0.0 reduce-scatter.5.cloned.1.call-update
  102.4 85.1 %reduce-scatter.5.cloned.1.call-done = bf16[64,1024]{1,0:T(8,128)(2,1)} async-done(((bf16[1024,1024]{1,0:T(8,128)(2,1)}), bf16[64,1024]{1,0:T(8,128)(2,1)}) %reduce-scatter.5.cloned.1.call-update) | async-done | bytes 131088 | tf_op jit(solution)/shard_map/reduce_scatter | solution.py:38
  (3 shorter events, 0.1 us)
Async XLA Ops:
  6.5 75.0 %copy-start = (bf16[1,512,2048]{2,1,0:T(8,128)(2,1)S(1)}, bf16[1,512,2048]{2,1,0:T(8,128)(2,1)}, u32[]{:S(2)}) copy-start(bf16[1,512,2048]{2,1,0:T(8,128)(2,1)} %param.12) | copy-start | bytes 6291460
  6.5 68.4 %all-gather.3.cloned.1.call-start = ((), (), s32[]{:S(2)}) async-start(), calls=%async_computation.2 | async-start | bytes 4325376 | tf_op jit(solution)/shard_map/all_gather | solution.py:24
  9.4 93.0 %reduce-scatter.3.cloned.1.call-start = ((), (), s32[]{:S(2)}) async-start(), calls=%async_computation.3 | async-start | bytes 6291456 | tf_op jit(solution)/shard_map/reduce_scatter | solution.py:37
  91.6 95.9 %reduce-scatter.5.cloned.1.call-start = ((), (), s32[]{:S(2)}) async-start(), calls=%async_computation.4 | async-start | bytes 2228224 | tf_op jit(solution)/shard_map/reduce_scatter | solution.py:38
Sparse Core Ops, SparseCore 0:
  10.2 64.7 all-gather.2
  91.7 10.6 reduce-scatter.2
  104.7 82.7 reduce-scatter.4

commit v2 on v0

--- a/solution.py
+++ b/solution.py
@@ -1,6 +1,10 @@
+import functools
+
 import jax
 import jax.numpy as jnp
 from jax import lax
+from jax.experimental import pallas as pl
+from jax.experimental.pallas import tpu as pltpu
 from jax.sharding import PartitionSpec as P
 
 TOP = 8
@@ -8,6 +12,10 @@
 
 
 EPSILON = 1e-06
+
+MESH = pl.DeviceIdType.MESH
+PLANE = 4
+DEPTH = 4
 
 
 def on_device(
@@ -72,6 +80,299 @@
     return jnp.sum(picked * gate_values[:, :, None], axis=1).astype(jnp.bfloat16)
 
 
+def plane_order(step, z):
+    if step == 0:
+        return z
+    if step == 1:
+        return z + 1 - 2 * (z % 2)
+    far = DEPTH - 1 - (DEPTH - 1) * (z // 2)
+    return far + (1 - 2 * (1 - z // 2)) * (DEPTH - 1 - step)
+
+
+def kernel(
+    expert_total, tokens_ref, gain_ref, gate_hbm, up_hbm, down_hbm, ids_ref, group_ref, weight_ref,
+    out_ref,
+    rows, gate_w, up_w, down_w, own_part, give, got, diag_out, diag_x, diag_y, x_out, y_out,
+    x_in, y_in, z_total, z_out, z_below, z_above,
+    w_sem, up_s, dn_s, z_r, gx_s, gx_r, gy_s, gy_r, dx_s, dx_r, dy_s, dy_r, sib_s, sib_r,
+    tp_s, tp_r, rdx_s, rdx_r, rdy_s, rdy_r, rx_s, rx_r, ry_s, ry_r, rz_s, rzb_r, rza_r,
+):
+    me = lax.axis_index("ep")
+    core = lax.axis_index("tp")
+    z, q = me // PLANE, me % PLANE
+    y, x = q // 2, q % 2
+    qx, qy, qd = y * 2 + 1 - x, (1 - y) * 2 + x, (1 - y) * 2 + 1 - x
+    x_peer, y_peer = {"ep": z * PLANE + qx}, {"ep": z * PLANE + qy}
+    up_peer, dn_peer = {"ep": me + PLANE}, {"ep": me - PLANE}
+    sibling = {"tp": 1 - core}
+    has_up, has_dn = z < DEPTH - 1, z > 0
+    half_rows, width = tokens_ref.shape[0] // 2, tokens_ref.shape[1]
+    sub = half_rows // 2
+    block = 2 * half_rows
+    part = width // 2
+    always = None
+    sent = []
+
+    weight_copies = [
+        pltpu.make_async_copy(src.at[0], dst, w_sem.at[i])
+        for i, (src, dst) in enumerate(((gate_hbm, gate_w), (up_hbm, up_w), (down_hbm, down_w)))
+    ]
+    for copy in weight_copies:
+        copy.start()
+
+    barrier = pltpu.get_barrier_semaphore()
+    for peer in (x_peer, y_peer, sibling):
+        pl.semaphore_signal(barrier, inc=1, device_id=peer, device_id_type=MESH)
+
+    @pl.when(has_up)
+    def _():
+        pl.semaphore_signal(barrier, inc=1, device_id=up_peer, device_id_type=MESH)
+
+    @pl.when(has_dn)
+    def _():
+        pl.semaphore_signal(barrier, inc=1, device_id=dn_peer, device_id_type=MESH)
+
+    def send(src, dst, send_sem, recv_sem, peer, when=always):
+        copy = pltpu.make_async_remote_copy(
+            src_ref=src, dst_ref=dst, send_sem=send_sem, recv_sem=recv_sem,
+            device_id=peer, device_id_type=MESH,
+        )
+        sent.append((copy, when))
+        if when is None:
+            copy.start()
+        else:
+            pl.when(when)(copy.start)
+
+    def arrive(dst, recv_sem):
+        pltpu.make_async_remote_copy(
+            src_ref=dst, dst_ref=dst, send_sem=recv_sem, recv_sem=recv_sem,
+            device_id=sibling, device_id_type=MESH,
+        ).wait_recv()
+
+    begin = pl.multiple_of(core * half_rows, half_rows)
+    values = tokens_ref[pl.ds(begin, half_rows), :].astype(jnp.float32)
+    scale = lax.rsqrt(jnp.mean(values * values, axis=-1, keepdims=True) + EPSILON)
+    normed = (values * scale * gain_ref[...]).astype(jnp.bfloat16)
+    lane = lax.broadcasted_iota(jnp.int32, (half_rows, 128), 1)
+    expert = lane % expert_total
+    ids = ids_ref[pl.ds(begin, half_rows), :]
+    weights = weight_ref[pl.ds(begin, half_rows), :]
+    groups = group_ref[pl.ds(begin, half_rows), :]
+    weights = weights / jnp.sum(weights, axis=1, keepdims=True)
+    gates = jnp.zeros((half_rows, 128), jnp.float32)
+    for k in range(TOP):
+        gates = gates + jnp.where(ids[:, k : k + 1] == expert, weights[:, k : k + 1], 0.0)
+    group_part = jnp.zeros((half_rows, 128), jnp.float32)
+    for g in range(groups.shape[1]):
+        group_part = jnp.where(expert // EXP_GRP == g, groups[:, g : g + 1], group_part)
+    gates = gates * group_part
+    high = gates.astype(jnp.bfloat16).astype(jnp.float32)
+    middle = (gates - high).astype(jnp.bfloat16).astype(jnp.float32)
+    low = gates - high - middle
+    third = lane // expert_total
+    tail = jnp.where(
+        third == 0, high, jnp.where(third == 1, middle, jnp.where(third == 2, low, 0.0))
+    ).astype(jnp.bfloat16)
+    for p in range(2):
+        rows[z, q, core, p, :, 0:width] = normed[p * sub : (p + 1) * sub]
+        rows[z, q, core, p, :, width:] = tail[p * sub : (p + 1) * sub]
+
+    pl.semaphore_wait(barrier, 3 + jnp.minimum(z, 1) + jnp.minimum(DEPTH - 1 - z, 1))
+
+    def own_column(step):
+        at = plane_order(step, z)
+        for p in range(2):
+            piece = rows.at[at, q, core, p]
+            if step > 0:
+                arrive(piece, z_r.at[at, p])
+            send(piece, piece, up_s.at[at, p], z_r.at[at, p], up_peer, has_up & (at <= z))
+            send(piece, piece, dn_s.at[at, p], z_r.at[at, p], dn_peer, has_dn & (at >= z))
+            send(piece, piece, gx_s.at[at, p], gx_r.at[at, p], x_peer)
+            send(piece, piece, gy_s.at[at, p], gy_r.at[at, p], y_peer)
+        to_sibling(at, q)
+
+    def to_sibling(at, column):
+        piece = rows.at[at, column, core]
+        send(piece, piece, sib_s.at[at, column], sib_r.at[at, column], sibling)
+
+    def neighbours(step):
+        at = plane_order(step, z)
+        arrive(rows.at[at, qx, core, 0], gx_r.at[at, 0])
+        piece = rows.at[at, qx, core, 0]
+        send(piece, piece, dy_s.at[at], dy_r.at[at], y_peer)
+        arrive(rows.at[at, qy, core, 1], gy_r.at[at, 1])
+        piece = rows.at[at, qy, core, 1]
+        send(piece, piece, dx_s.at[at], dx_r.at[at], x_peer)
+        arrive(rows.at[at, qx, core, 1], gx_r.at[at, 1])
+        to_sibling(at, qx)
+        arrive(rows.at[at, qy, core, 0], gy_r.at[at, 0])
+        to_sibling(at, qy)
+
+    def diagonal(step):
+        at = plane_order(step, z)
+        arrive(rows.at[at, qd, core, 0], dy_r.at[at])
+        arrive(rows.at[at, qd, core, 1], dx_r.at[at])
+        to_sibling(at, qd)
+
+    mine = pl.multiple_of(core * part, part)
+    other = pl.multiple_of((1 - core) * part, part)
+
+    def compute(step):
+        at = plane_order(step, z)
+        for column in range(PLANE):
+            arrive(rows.at[at, column, 1 - core], sib_r.at[at, column])
+        if step == 0:
+            for copy in weight_copies:
+                copy.wait()
+        count = PLANE * block
+        taken = rows[at, :, :, :, :, 0:width].reshape(count, width)
+        gate_acts = jnp.dot(taken, gate_w[...], preferred_element_type=jnp.float32)
+        up_acts = jnp.dot(taken, up_w[...], preferred_element_type=jnp.float32)
+        hidden = (gate_acts / (1.0 + jnp.exp(-gate_acts)) * up_acts).astype(jnp.bfloat16)
+        tails = rows[at, :, :, :, :, width:].reshape(count, 128).astype(jnp.float32)
+        lanes = lax.broadcasted_iota(jnp.int32, (count, 128), 1)
+        wanted = (lanes % expert_total == me) & (lanes < 3 * expert_total)
+        gate = jnp.sum(jnp.where(wanted, tails, 0.0), axis=1, keepdims=True)
+        theirs = jnp.dot(hidden, down_w[:, pl.ds(other, part)], preferred_element_type=jnp.float32)
+        give[at] = (theirs * gate).astype(jnp.bfloat16).reshape(PLANE, block, part)
+        send(give.at[at], got.at[at], tp_s.at[at], tp_r.at[at], sibling)
+        ours = jnp.dot(hidden, down_w[:, pl.ds(mine, part)], preferred_element_type=jnp.float32)
+        own_part[at] = (ours * gate).reshape(PLANE, block, part)
+
+    def pair_sum(at, column):
+        return own_part[at, column] + got[at, column].astype(jnp.float32)
+
+    def give_diagonal(step):
+        at = plane_order(step, z)
+        arrive(got.at[at], tp_r.at[at])
+        diag_out[at] = pair_sum(at, qd).astype(jnp.bfloat16).reshape(2, half_rows, part)
+        send(diag_out.at[at, 0], diag_x.at[at], rdx_s.at[at], rdx_r.at[at], x_peer)
+        send(diag_out.at[at, 1], diag_y.at[at], rdy_s.at[at], rdy_r.at[at], y_peer)
+
+    def give_neighbours(step):
+        at = plane_order(step, z)
+        arrive(diag_x.at[at], rdx_r.at[at])
+        total = pair_sum(at, qy)
+        y_out[at, 0:half_rows] = (
+            total[0:half_rows] + diag_x[at].astype(jnp.float32)
+        ).astype(jnp.bfloat16)
+        y_out[at, half_rows:] = total[half_rows:].astype(jnp.bfloat16)
+        send(y_out.at[at], y_in.at[at], ry_s.at[at], ry_r.at[at], y_peer)
+        arrive(diag_y.at[at], rdy_r.at[at])
+        total = pair_sum(at, qx)
+        x_out[at, 0:half_rows] = total[0:half_rows].astype(jnp.bfloat16)
+        x_out[at, half_rows:] = (
+            total[half_rows:] + diag_y[at].astype(jnp.float32)
+        ).astype(jnp.bfloat16)
+        send(x_out.at[at], x_in.at[at], rx_s.at[at], rx_r.at[at], x_peer)
+
+    def give_column(step):
+        at = plane_order(step, z)
+        arrive(x_in.at[at], rx_r.at[at])
+        arrive(y_in.at[at], ry_r.at[at])
+        z_total[...] = (
+            pair_sum(at, q) + x_in[at].astype(jnp.float32) + y_in[at].astype(jnp.float32)
+        )
+
+        @pl.when(has_dn & (at >= z))
+        def _():
+            arrive(z_below.at[at], rzb_r.at[at])
+            z_total[...] += z_below[at].astype(jnp.float32)
+
+        @pl.when(has_up & (at <= z))
+        def _():
+            arrive(z_above.at[at], rza_r.at[at])
+            z_total[...] += z_above[at].astype(jnp.float32)
+
+        if step == 0:
+            out_ref[...] = z_total[...].astype(jnp.bfloat16)
+        else:
+            z_out[at] = z_total[...].astype(jnp.bfloat16)
+            send(z_out.at[at], z_below.at[at], rz_s.at[at], rzb_r.at[at], up_peer, at > z)
+            send(z_out.at[at], z_above.at[at], rz_s.at[at], rza_r.at[at], dn_peer, at < z)
+
+    own_column(0)
+    own_column(1)
+    neighbours(0)
+    own_column(2)
+    neighbours(1)
+    diagonal(0)
+    own_column(3)
+    neighbours(2)
+    diagonal(1)
+    compute(0)
+    neighbours(3)
+    diagonal(2)
+    compute(1)
+    give_diagonal(0)
+    compute(2)
+    give_diagonal(1)
+    diagonal(3)
+    compute(3)
+    give_diagonal(2)
+    give_diagonal(3)
+    give_neighbours(2)
+    give_neighbours(3)
+    give_neighbours(1)
+    give_column(3)
+    give_neighbours(0)
+    give_column(2)
+    give_column(1)
+    give_column(0)
+
+    for copy, when in sent:
+        if when is None:
+            copy.wait_send()
+        else:
+            pl.when(when)(copy.wait_send)
+
+
+def fused(
+    tokens_in, norm_gain, gate_proj, up_proj, down_proj, route_ids, group_weight, expert_weight
+):
+    token_count, model_width = tokens_in.shape
+    expert_total = gate_proj.shape[0] * lax.axis_size("ep")
+    hidden_width = gate_proj.shape[2]
+    part = model_width // 2
+    half_rows = token_count // 2
+    bf16, f32 = jnp.bfloat16, jnp.float32
+    dma = pltpu.SemaphoreType.DMA
+    vmem, hbm = pl.BlockSpec(memory_space=pltpu.VMEM), pl.BlockSpec(memory_space=pl.ANY)
+    blocks = pltpu.VMEM((DEPTH, token_count, part), bf16)
+    halves = pltpu.VMEM((DEPTH, half_rows, part), bf16)
+    return pl.pallas_call(
+        functools.partial(kernel, expert_total),
+        out_shape=jax.ShapeDtypeStruct((token_count, part), bf16),
+        in_specs=[vmem, vmem, hbm, hbm, hbm, vmem, vmem, vmem],
+        out_specs=vmem,
+        scratch_shapes=[
+            pltpu.VMEM((DEPTH, PLANE, 2, 2, half_rows // 2, model_width + 128), bf16),
+            pltpu.VMEM((model_width, hidden_width), bf16),
+            pltpu.VMEM((model_width, hidden_width), bf16),
+            pltpu.VMEM((hidden_width, model_width), bf16),
+            pltpu.VMEM((DEPTH, PLANE, token_count, part), f32),
+            pltpu.VMEM((DEPTH, PLANE, token_count, part), bf16),
+            pltpu.VMEM((DEPTH, PLANE, token_count, part), bf16),
+            pltpu.VMEM((DEPTH, 2, half_rows, part), bf16),
+            halves, halves, blocks, blocks, blocks, blocks,
+            pltpu.VMEM((token_count, part), f32),
+            blocks, blocks, blocks,
+            dma((3,)),
+            dma((DEPTH, 2)), dma((DEPTH, 2)), dma((DEPTH, 2)),
+            dma((DEPTH, 2)), dma((DEPTH, 2)), dma((DEPTH, 2)), dma((DEPTH, 2)),
+            dma((DEPTH,)), dma((DEPTH,)), dma((DEPTH,)), dma((DEPTH,)),
+            dma((DEPTH, PLANE)), dma((DEPTH, PLANE)),
+        ]
+        + [dma((DEPTH,))] * 13,
+        compiler_params=pltpu.CompilerParams(
+            collective_id=0, has_side_effects=True, vmem_limit_bytes=60 * 1024 * 1024
+        ),
+    )(
+        tokens_in, norm_gain.reshape(1, model_width), gate_proj, up_proj, down_proj,
+        route_ids, group_weight, expert_weight,
+    )
+
+
 def solution(mesh):
     in_specs = (
         P(("grp", "ep"), None),
@@ -84,6 +385,7 @@
         P(("grp", "ep"), None),
     )
     out_specs = P(("grp", "ep"), "tp")
+    relayed = mesh.shape["ep"] == PLANE * DEPTH and mesh.shape["tp"] == 2
     return jax.shard_map(
-        on_device, mesh=mesh, in_specs=in_specs, out_specs=out_specs, check_vma=False
-    )
+        fused if relayed else on_device, mesh=mesh, in_specs=in_specs, out_specs=out_specs, check_vma=False
+    )

time: 174 us -> 66.6 us (0.38)
  the two profiles are of different devices: /device:TPU:12 before, /device:TPU:0 now
where the time goes in v2:
time: 66.6 us; the launch traced here: 66.4 us
  Pallas kernels  60.7 us (91%)
  local copies, waits for them, and re-layouts  5.69 us (9%)
    pallas_call x1, Pallas kernels, fused(): pl.pallas_call(functools.partial(kernel, expert_total), out_shape=jax.Sha...  60.7 us
    unnamed x4, local copies, waits for them, and re-layouts  5.69 us

profile of v2, /device:TPU:0, one launch (start us, length us, event | category | flops | bytes accessed | tf_op | source)
XLA Modules:
  0.0 66.4 jit_solution(15028364266204125201)
XLA Ops:
  0.0 1.4 %copy.9.ids_ref = s32[64,8]{1,0:T(8,128)} copy(s32[64,8]{0,1:T(8,128)} %param.13) | data formatting | bytes 4096 | tf_op args[5]
  1.4 1.4 %copy.10.group_ref = f32[64,2]{1,0:T(8,128)} copy(f32[64,2]{0,1:T(2,128)} %param.14) | data formatting | bytes 1024 | tf_op args[6]
  2.7 1.4 %copy.11.weight_ref = f32[64,8]{1,0:T(8,128)} copy(f32[64,8]{0,1:T(8,128)} %param.15) | data formatting | bytes 4096 | tf_op args[7]
  4.1 60.7 %shard_map.82 = bf16[64,1024]{1,0:T(8,128)(2,1)} custom-call(bf16[64,2048]{1,0:T(8,128)(2,1)} %tokens_ref.1, f32[1,2048]{1,0:T(1,128)} %bitcast.1, bf16[1,2048,512]{2,1,0:T(8,128)(2,1)} %gate_hbm.1, bf16[1,2048,512]{2,1,0:T(8,128)(2,1)} %up_hbm.1, bf16[1,512,2048]{2,1,0:T(8,128)(2,1)} %down_hbm.1, s32[64,8]{1,0:T(8,128)} %copy.9.ids_ref, ...), custom_call_target="tpu_custom_call" | custom-call | tf_op jit(solution)/shard_map/pallas_call | solution.py:343
  64.8 1.6 %copy.13 = bf16[64,1024]{1,0:T(8,128)(2,1)} copy(bf16[64,1024]{1,0:T(8,128)(2,1)} %shard_map.82) | data formatting | bytes 262144

commit v3 on v2

--- a/solution.py
+++ b/solution.py
@@ -155,9 +155,11 @@
     normed = (values * scale * gain_ref[...]).astype(jnp.bfloat16)
     lane = lax.broadcasted_iota(jnp.int32, (half_rows, 128), 1)
     expert = lane % expert_total
-    ids = ids_ref[pl.ds(begin, half_rows), :]
-    weights = weight_ref[pl.ds(begin, half_rows), :]
-    groups = group_ref[pl.ds(begin, half_rows), :]
+    picks = [
+        jnp.where(core == 0, turned[0:half_rows], turned[half_rows:])
+        for turned in (ids_ref[...].T, weight_ref[...].T, group_ref[...].T)
+    ]
+    ids, weights, groups = picks
     weights = weights / jnp.sum(weights, axis=1, keepdims=True)
     gates = jnp.zeros((half_rows, 128), jnp.float32)
     for k in range(TOP):
@@ -239,65 +241,72 @@
         ours = jnp.dot(hidden, down_w[:, pl.ds(mine, part)], preferred_element_type=jnp.float32)
         own_part[at] = (ours * gate).reshape(PLANE, block, part)
 
-    def pair_sum(at, column):
-        return own_part[at, column] + got[at, column].astype(jnp.float32)
+    def pair_sum(at, column, half):
+        held = pl.ds(half * half_rows, half_rows)
+        return own_part[at, column, held] + got[at, column, held].astype(jnp.float32)
 
     def give_diagonal(step):
         at = plane_order(step, z)
         arrive(got.at[at], tp_r.at[at])
-        diag_out[at] = pair_sum(at, qd).astype(jnp.bfloat16).reshape(2, half_rows, part)
-        send(diag_out.at[at, 0], diag_x.at[at], rdx_s.at[at], rdx_r.at[at], x_peer)
-        send(diag_out.at[at, 1], diag_y.at[at], rdy_s.at[at], rdy_r.at[at], y_peer)
+        for half, (dst, send_sem, recv_sem, peer) in enumerate(
+            ((diag_x, rdx_s, rdx_r, x_peer), (diag_y, rdy_s, rdy_r, y_peer))
+        ):
+            diag_out[at, half] = pair_sum(at, qd, half).astype(jnp.bfloat16)
+            send(diag_out.at[at, half], dst.at[at], send_sem.at[at], recv_sem.at[at], peer)
+        y_out[at, 1] = pair_sum(at, qy, 1).astype(jnp.bfloat16)
+        send(y_out.at[at, 1], y_in.at[at, 1], ry_s.at[at, 1], ry_r.at[at, 1], y_peer)
+        x_out[at, 0] = pair_sum(at, qx, 0).astype(jnp.bfloat16)
+        send(x_out.at[at, 0], x_in.at[at, 0], rx_s.at[at, 0], rx_r.at[at, 0], x_peer)
 
     def give_neighbours(step):
         at = plane_order(step, z)
         arrive(diag_x.at[at], rdx_r.at[at])
-        total = pair_sum(at, qy)
-        y_out[at, 0:half_rows] = (
-            total[0:half_rows] + diag_x[at].astype(jnp.float32)
-        ).astype(jnp.bfloat16)
-        y_out[at, half_rows:] = total[half_rows:].astype(jnp.bfloat16)
-        send(y_out.at[at], y_in.at[at], ry_s.at[at], ry_r.at[at], y_peer)
+        y_out[at, 0] = (pair_sum(at, qy, 0) + diag_x[at].astype(jnp.float32)).astype(jnp.bfloat16)
+        send(y_out.at[at, 0], y_in.at[at, 0], ry_s.at[at, 0], ry_r.at[at, 0], y_peer)
         arrive(diag_y.at[at], rdy_r.at[at])
-        total = pair_sum(at, qx)
-        x_out[at, 0:half_rows] = total[0:half_rows].astype(jnp.bfloat16)
-        x_out[at, half_rows:] = (
-            total[half_rows:] + diag_y[at].astype(jnp.float32)
-        ).astype(jnp.bfloat16)
-        send(x_out.at[at], x_in.at[at], rx_s.at[at], rx_r.at[at], x_peer)
+        x_out[at, 1] = (pair_sum(at, qx, 1) + diag_y[at].astype(jnp.float32)).astype(jnp.bfloat16)
+        send(x_out.at[at, 1], x_in.at[at, 1], rx_s.at[at, 1], rx_r.at[at, 1], x_peer)
 
     def give_column(step):
         at = plane_order(step, z)
-        arrive(x_in.at[at], rx_r.at[at])
-        arrive(y_in.at[at], ry_r.at[at])
+        for half in range(2):
+            arrive(x_in.at[at, half], rx_r.at[at, half])
+            arrive(y_in.at[at, half], ry_r.at[at, half])
+            add_planes(step, at, half)
+
+    def add_planes(step, at, half):
         z_total[...] = (
-            pair_sum(at, q) + x_in[at].astype(jnp.float32) + y_in[at].astype(jnp.float32)
+            pair_sum(at, q, half)
+            + x_in[at, half].astype(jnp.float32)
+            + y_in[at, half].astype(jnp.float32)
         )
 
         @pl.when(has_dn & (at >= z))
         def _():
-            arrive(z_below.at[at], rzb_r.at[at])
-            z_total[...] += z_below[at].astype(jnp.float32)
+            arrive(z_below.at[at, half], rzb_r.at[at, half])
+            z_total[...] += z_below[at, half].astype(jnp.float32)
 
         @pl.when(has_up & (at <= z))
         def _():
-            arrive(z_above.at[at], rza_r.at[at])
-            z_total[...] += z_above[at].astype(jnp.float32)
-
+            arrive(z_above.at[at, half], rza_r.at[at, half])
+            z_total[...] += z_above[at, half].astype(jnp.float32)
+
+        piece = z_out.at[at, half]
         if step == 0:
-            out_ref[...] = z_total[...].astype(jnp.bfloat16)
+            out_ref[half * half_rows : (half + 1) * half_rows] = z_total[...].astype(jnp.bfloat16)
         else:
-            z_out[at] = z_total[...].astype(jnp.bfloat16)
-            send(z_out.at[at], z_below.at[at], rz_s.at[at], rzb_r.at[at], up_peer, at > z)
-            send(z_out.at[at], z_above.at[at], rz_s.at[at], rza_r.at[at], dn_peer, at < z)
+            z_out[at, half] = z_total[...].astype(jnp.bfloat16)
+            below, above = z_below.at[at, half], z_above.at[at, half]
+            send(piece, below, rz_s.at[at, half], rzb_r.at[at, half], up_peer, at > z)
+            send(piece, above, rz_s.at[at, half], rza_r.at[at, half], dn_peer, at < z)
 
     own_column(0)
     own_column(1)
+    own_column(2)
     neighbours(0)
-    own_column(2)
+    own_column(3)
     neighbours(1)
     diagonal(0)
-    own_column(3)
     neighbours(2)
     diagonal(1)
     compute(0)
@@ -309,14 +318,14 @@
     give_diagonal(1)
     diagonal(3)
     compute(3)
+    give_diagonal(3)
     give_diagonal(2)
-    give_diagonal(3)
+    give_neighbours(3)
     give_neighbours(2)
-    give_neighbours(3)
+    give_column(3)
     give_neighbours(1)
-    give_column(3)
+    give_column(2)
     give_neighbours(0)
-    give_column(2)
     give_column(1)
     give_column(0)
 
@@ -338,7 +347,7 @@
     bf16, f32 = jnp.bfloat16, jnp.float32
     dma = pltpu.SemaphoreType.DMA
     vmem, hbm = pl.BlockSpec(memory_space=pltpu.VMEM), pl.BlockSpec(memory_space=pl.ANY)
-    blocks = pltpu.VMEM((DEPTH, token_count, part), bf16)
+    blocks = pltpu.VMEM((DEPTH, 2, half_rows, part), bf16)
     halves = pltpu.VMEM((DEPTH, half_rows, part), bf16)
     return pl.pallas_call(
         functools.partial(kernel, expert_total),
@@ -355,7 +364,7 @@
             pltpu.VMEM((DEPTH, PLANE, token_count, part), bf16),
             pltpu.VMEM((DEPTH, 2, half_rows, part), bf16),
             halves, halves, blocks, blocks, blocks, blocks,
-            pltpu.VMEM((token_count, part), f32),
+            pltpu.VMEM((half_rows, part), f32),
             blocks, blocks, blocks,
             dma((3,)),
             dma((DEPTH, 2)), dma((DEPTH, 2)), dma((DEPTH, 2)),
@@ -363,13 +372,14 @@
             dma((DEPTH,)), dma((DEPTH,)), dma((DEPTH,)), dma((DEPTH,)),
             dma((DEPTH, PLANE)), dma((DEPTH, PLANE)),
         ]
-        + [dma((DEPTH,))] * 13,
+        + [dma((DEPTH,))] * 6
+        + [dma((DEPTH, 2))] * 7,
         compiler_params=pltpu.CompilerParams(
             collective_id=0, has_side_effects=True, vmem_limit_bytes=60 * 1024 * 1024
         ),
     )(
         tokens_in, norm_gain.reshape(1, model_width), gate_proj, up_proj, down_proj,
-        route_ids, group_weight, expert_weight,
+        route_ids.T, group_weight.T, expert_weight.T,
     )
 
 

time: 66.6 us -> 60.9 us (0.914)
  local copies, waits for them, and re-layouts: 5.69 us -> 1.57 us
  Pallas kernels: 60.7 us -> 59.2 us
    unnamed x4 -> x1, local copies, waits for them, and re-layouts: 5.69 us -> 1.57 us
    pallas_call x1, Pallas kernels: 60.7 us -> 59.2 us  [fused(): pl.pallas_call(functools.partial(kernel, expert_total), out_shape=jax.Sha...]
where the time goes in v3:
time: 60.9 us; the launch traced here: 60.8 us
  Pallas kernels  59.2 us (97%)
  local copies, waits for them, and re-layouts  1.57 us (3%)
    pallas_call x1, Pallas kernels, fused(): pl.pallas_call(functools.partial(kernel, expert_total), out_shape=jax.Sha...  59.2 us
    unnamed x1, local copies, waits for them, and re-layouts  1.57 us

profile of v3, /device:TPU:0, one launch (start us, length us, event | category | flops | bytes accessed | tf_op | source)
XLA Modules:
  0.0 60.8 jit_solution(15136015929721934847)
XLA Ops:
  0.0 59.2 %shard_map.82 = bf16[64,1024]{1,0:T(8,128)(2,1)} custom-call(bf16[64,2048]{1,0:T(8,128)(2,1)} %tokens_ref.1, f32[1,2048]{1,0:T(1,128)} %bitcast.4, bf16[1,2048,512]{2,1,0:T(8,128)(2,1)} %gate_hbm.1, bf16[1,2048,512]{2,1,0:T(8,128)(2,1)} %up_hbm.1, bf16[1,512,2048]{2,1,0:T(8,128)(2,1)} %down_hbm.1, s32[8,64]{1,0:T(8,128)} %bitcast.5, f32[2,64]{1,0:T(2,128)} %bitcast.7, ...), custom_call_target="tpu_custom_call" | custom-call | tf_op jit(solution)/shard_map/pallas_call | solution.py:352
  59.2 1.6 %copy.10 = bf16[64,1024]{1,0:T(8,128)(2,1)} copy(bf16[64,1024]{1,0:T(8,128)(2,1)} %shard_map.82) | data formatting | bytes 262144
